TPU v7x, 32 devices: a whole 2x2x4 slice. The times are simulated.
32 devices in a mesh: grp: 2 (over x), tp: 16 (over z, y, core).
Axes of the slice: x: 2, y: 2, z: 4, core: 2. Of those that a mesh axis runs over, the one named last changes fastest.
Arguments:
- residual_channel: bfloat16 [256, 8, 4096], P('grp', None, 'tp'), parts along dimension 0, may hold values from -18 to 18, as said below
- prior_block_multiplier: float32 [2, 4096], replicated, may hold values from 0.1 to 1.9
- probe_map_matrix: bfloat16 [2, 4096, 2048], P(None, None, 'tp'), may hold values from -0.09375 to 0.09375
- lookup_map_matrix: bfloat16 [2, 4096, 2048], P(None, None, 'tp'), may hold values from -0.09375 to 0.09375
- content_map_matrix: bfloat16 [2, 4096, 2048], P(None, None, 'tp'), may hold values from -0.09375 to 0.09375
- emission_valve_matrix: bfloat16 [2, 4096, 2048], P(None, None, 'tp'), may hold values from -0.09375 to 0.09375
- forgetting_map_matrix: bfloat16 [2, 4096, 32], replicated, may hold values from -0.09375 to 0.09375
- insertion_rate_matrix: bfloat16 [2, 4096, 32], replicated, may hold values from -0.09375 to 0.09375
- forgetting_magnitude_exponent: float32 [2, 32], P(None, 'tp'), may hold values from -4.6 to -1.2
- channel_forgetting_offset: float32 [2, 32], P(None, 'tp'), may hold values from -2 to 1
- surplus_forgetting_amounts: float32 [2, 256, 8, 32], P(None, 'grp', None, 'tp'), parts along dimension 1, may hold values from -0.7 to 0
- readout_rescale_multiplier: float32 [2, 2048], P(None, 'tp'), may hold values from 0.1 to 1.9
- emission_map_matrix: bfloat16 [2, 2048, 4096], P(None, None, 'tp'), may hold values from -2 to 2
- post_mixing_multiplier: float32 [2, 4096], replicated, may hold values from 0.1 to 1.9
- recurrent_matrices: float32 [2, 256, 32, 4096], P(None, 'grp', 'tp'), parts along dimension 1, may hold values from -6 to 6
Outputs:
- new_stream: bfloat16 [256, 8, 4096], P('grp', None, 'tp'), parts along dimension 0
- new_memory: float32 [2, 256, 32, 4096], P(None, 'grp', 'tp'), parts along dimension 1
There are 2 independent parts, one for each index of `grp`. A program takes and returns all parts, laid end to end along the dimension named above; an argument that names none is the same for every part. Nothing has to cross between parts.
Inputs may be any that keep to these rules, and one draw needn't show every extreme that they name: `residual_channel`: column scales of the features differ widely.
All inputs are finite; a program needn't handle non-finite values.
Results may differ from a plain program's by a relative error of at most 0.0081.
Values may be sent and summed in bfloat16 or wider, within the bound.
A program may use at most 192 MiB of HBM per device.

v0:
```python
import jax
import jax.numpy as jnp
from jax import lax
from jax.sharding import PartitionSpec as P

D = 4096
HEAD_DIM = 64
LAYERS = 2
EPS = 1e-06
HIGH = lax.Precision.HIGHEST


def solve_lower(a_mat, right_side):
    length = right_side.shape[-2]
    solved_rows = []
    for row_at in range(length):
        current_row = right_side[..., row_at, :]
        for col_at in range(row_at):
            current_row = current_row - a_mat[..., row_at, col_at][..., None] * solved_rows[col_at]
        solved_rows.append(current_row)
    return jnp.stack(solved_rows, axis=-2)


def delta_block(queries, key_rows, values, forgetting_exponent_amount, strength, matrix_state):
    length = queries.shape[2]
    causal = jnp.tril(jnp.ones((length, length), bool))
    strict = jnp.tril(jnp.ones((length, length), bool), -1)
    cumulative = jnp.cumsum(forgetting_exponent_amount, axis=-1)
    decay_mat = jnp.where(
        causal,
        jnp.exp(jnp.where(causal, cumulative[..., :, None] - cumulative[..., None, :], 0.0)),
        0.0,
    )
    key_gram = jnp.einsum("bhtd,bhsd->bhts", key_rows, key_rows, precision=HIGH)
    a_mat = jnp.where(strict, strength[..., :, None] * decay_mat * key_gram, 0.0)
    right_side = jnp.concatenate(
        [strength[..., None] * values, (strength * jnp.exp(cumulative))[..., None] * key_rows],
        axis=-1,
    )
    solved = solve_lower(a_mat, right_side)
    width_v = values.shape[-1]
    update = solved[..., :width_v] - jnp.einsum(
        "bhtk,bhkv->bhtv", solved[..., width_v:], matrix_state, precision=HIGH
    )
    scores = jnp.einsum("bhtd,bhsd->bhts", queries, key_rows, precision=HIGH) * decay_mat
    output = jnp.exp(cumulative)[..., None] * jnp.einsum(
        "bhtk,bhkv->bhtv", queries, matrix_state, precision=HIGH
    )
    output = output + jnp.einsum("bhts,bhsv->bhtv", scores, update, precision=HIGH)
    final_log = cumulative[..., -1:]
    revised_memory_matrix = jnp.exp(final_log)[..., None] * matrix_state + jnp.einsum(
        "bhsk,bhsv->bhkv",
        key_rows * jnp.exp(final_log - cumulative)[..., None],
        update,
        precision=HIGH,
    )
    return (output, revised_memory_matrix)


def unit_rows(matrix):
    return matrix * lax.rsqrt(jnp.sum(matrix * matrix, axis=-1, keepdims=True) + EPS)


def token_blender(
    mapped_token_vectors,
    magnitude_exponent,
    offset_terms_array,
    surplus_forgetting_exponent,
    multiplier_terms_array,
    incoming_memory_matrix,
    batch_total,
    generation_round_total,
):
    rounded = [
        lax.optimization_barrier(part_sum.astype(jnp.bfloat16)).astype(jnp.float32)
        for part_sum in mapped_token_vectors
    ]
    queries, keys_raw, values_raw, gate_raw, decay_pre, strength_pre = rounded
    head_count = incoming_memory_matrix.shape[1]

    def to_heads(matrix):
        return matrix.reshape(batch_total, generation_round_total, head_count, HEAD_DIM).transpose(
            0, 2, 1, 3
        )

    def per_head(matrix):
        return matrix.reshape(batch_total, generation_round_total, head_count).transpose(0, 2, 1)

    queries = unit_rows(jax.nn.silu(to_heads(queries))) * HEAD_DIM ** (-0.5)
    key_rows = unit_rows(jax.nn.silu(to_heads(keys_raw)))
    values = jax.nn.silu(to_heads(values_raw))
    forgetting_exponent_amount = -jnp.exp(magnitude_exponent)[None, :, None] * jax.nn.softplus(
        per_head(decay_pre) + offset_terms_array[None, :, None]
    )
    forgetting_exponent_amount = forgetting_exponent_amount + surplus_forgetting_exponent.transpose(
        0, 2, 1
    )
    strength = jax.nn.sigmoid(per_head(strength_pre))
    matrix_state = incoming_memory_matrix.reshape(batch_total, head_count, HEAD_DIM, HEAD_DIM)
    output, revised_memory_matrix = delta_block(
        queries, key_rows, values, forgetting_exponent_amount, strength, matrix_state
    )
    normed = output * lax.rsqrt(jnp.mean(output * output, axis=-1, keepdims=True) + EPS)
    normed = (
        normed
        * multiplier_terms_array.reshape(head_count, HEAD_DIM)[None, :, None, :]
        * jax.nn.silu(to_heads(gate_raw))
    )
    blended_token_vectors = (
        normed.transpose(0, 2, 1, 3)
        .reshape(batch_total * generation_round_total, head_count * HEAD_DIM)
        .astype(jnp.bfloat16)
    )
    return (
        blended_token_vectors,
        revised_memory_matrix.reshape(batch_total, head_count, HEAD_DIM * HEAD_DIM),
    )


def project(portion, weights):
    return tuple(
        (jnp.dot(portion, weight, preferred_element_type=jnp.float32) for weight in weights)
    )


def out_project(blended_token_vectors, weight_rows):
    return jnp.dot(
        lax.all_gather(blended_token_vectors, "tp", axis=1, tiled=True),
        weight_rows,
        preferred_element_type=jnp.float32,
    ).astype(jnp.bfloat16)


def post_residual(widened, mixed_out, multiplier_terms_array, complete):
    mixed_wide = lax.optimization_barrier(mixed_out).astype(jnp.float32)
    squares = jnp.sum(mixed_wide * mixed_wide, axis=-1)
    if not complete:
        squares = lax.psum(squares, "tp")
    post_rms = lax.rsqrt(squares / D + EPS)[:, None]
    return lax.optimization_barrier(
        (widened + mixed_wide * post_rms * multiplier_terms_array).astype(jnp.bfloat16)
    )


def local(
    residual_channel,
    prior_block_multiplier,
    probe_map_matrix,
    lookup_map_matrix,
    content_map_matrix,
    emission_valve_matrix,
    forgetting_map_matrix,
    insertion_rate_matrix,
    forgetting_magnitude_exponent,
    channel_forgetting_offset,
    surplus_forgetting_amounts,
    readout_rescale_multiplier,
    emission_map_matrix,
    post_mixing_multiplier,
    recurrent_matrices,
):
    batch_total, generation_round_total, own_width = residual_channel.shape
    head_count = recurrent_matrices.shape[2]
    row_count = batch_total * generation_round_total
    col_offset = lax.axis_index("tp") * own_width
    head_offset = lax.axis_index("tp") * head_count
    new_states = []

    def mix_layer(mapped_token_vectors, block_index_number):
        blended_token_vectors, revised_memory_matrix = token_blender(
            mapped_token_vectors,
            forgetting_magnitude_exponent[block_index_number],
            channel_forgetting_offset[block_index_number],
            surplus_forgetting_amounts[block_index_number],
            readout_rescale_multiplier[block_index_number],
            recurrent_matrices[block_index_number],
            batch_total,
            generation_round_total,
        )
        new_states.append(revised_memory_matrix)
        return out_project(blended_token_vectors, emission_map_matrix[block_index_number])

    def own_cols(matrix):
        return lax.dynamic_slice_in_dim(matrix, col_offset, own_width, matrix.ndim - 1)

    whole_rows = lax.all_gather(
        residual_channel.reshape(row_count, own_width), "tp", axis=1, tiled=True
    )
    current = whole_rows
    for block_index_number in range(LAYERS):
        widened = whole_rows.astype(jnp.float32)
        inv_rms = lax.rsqrt(jnp.mean(widened * widened, axis=-1, keepdims=True) + EPS)
        hidden = (widened * inv_rms * prior_block_multiplier[block_index_number]).astype(
            jnp.bfloat16
        )
        weights = (
            probe_map_matrix[block_index_number],
            lookup_map_matrix[block_index_number],
            content_map_matrix[block_index_number],
            emission_valve_matrix[block_index_number],
            lax.dynamic_slice_in_dim(
                forgetting_map_matrix[block_index_number], head_offset, head_count, 1
            ),
            lax.dynamic_slice_in_dim(
                insertion_rate_matrix[block_index_number], head_offset, head_count, 1
            ),
        )
        mapped_token_vectors = project(hidden, weights)
        mixed_out = mix_layer(mapped_token_vectors, block_index_number)
        if block_index_number < LAYERS - 1:
            gathered = lax.all_gather(mixed_out, "tp", axis=1, tiled=True)
            whole_rows = post_residual(
                widened, gathered, post_mixing_multiplier[block_index_number], True
            )
        else:
            current = post_residual(
                own_cols(widened),
                mixed_out,
                own_cols(post_mixing_multiplier[block_index_number]),
                False,
            )
    return (
        current.reshape(batch_total, generation_round_total, own_width),
        jnp.stack(new_states, axis=0),
    )


def solution(mesh):
    return jax.shard_map(
        local,
        mesh=mesh,
        in_specs=(
            P("grp", None, "tp"),
            P(),
            P(None, None, "tp"),
            P(None, None, "tp"),
            P(None, None, "tp"),
            P(None, None, "tp"),
            P(),
            P(),
            P(None, "tp"),
            P(None, "tp"),
            P(None, "grp", None, "tp"),
            P(None, "tp"),
            P(None, None, "tp"),
            P(),
            P(None, "grp", "tp", None),
        ),
        out_specs=(P("grp", None, "tp"), P(None, "grp", "tp", None)),
        check_vma=False,
    )
```

profile of v0, /device:TPU:0, one launch (start us, length us, event | category | flops | bytes accessed | tf_op | source)
XLA Modules:
  0.0 673.6 jit_solution(834577331812609737)
XLA Ops:
  11.3 14.3 %fusion.190 = (f32[1,128,2,4096]{3,2,1,0:T(2,128)}, f32[1,128,2,4096]{3,2,1,0:T(2,128)}) fusion(f32[2,128,2,4096]{3,2,1,0:T(2,128)} %param.29), kind=kLoop, calls=%fused_computation.324 | loop fusion | bytes 16777216 | tf_op jit(solution)/shard_map/slice | solution.py:176
  25.6 7.4 %copy.607 = f32[1,128,2,4096]{1,3,2,0:T(8,128)} copy(f32[1,128,2,4096]{3,2,1,0:T(2,128)} %get-tuple-element.41) | data formatting | bytes 8388608
  33.1 9.3 %copy.482 = f32[128,2,64,64]{3,2,1,0:T(8,128)} copy(f32[128,2,64,64]{0,3,2,1:T(8,128)} %bitcast.322) | data formatting | bytes 8388608 | tf_op jit(solution)/shard_map/reshape;squeeze | solution.py:99
  44.6 46.0 %all-gather.5.cloned.1.call-done = bf16[1024,4096]{1,0:T(8,128)(2,1)} async-done(((bf16[1024,256]{1,0:T(8,128)(2,1)}), bf16[1024,4096]{1,0:T(8,128)(2,1)}) %all-gather.5.cloned.1.call-update) | async-done | bytes 8388624 | tf_op jit(solution)/shard_map/all_gather | solution.py:186
  95.7 10.5 %fusion.4 = bf16[1024,4096]{1,0:T(8,128)(2,1)} fusion(bf16[1024,4096]{1,0:T(8,128)(2,1)} %all-gather.5.cloned.1.call-done, f32[4096]{0:T(1024)S(1)} %bitcast.336, f32[1024]{0:T(1024)S(1)} %add_rsqrt_fusion.7), kind=kLoop, calls=%fused_computation.9 | loop fusion | flops 16777216 | bytes 16797696 | tf_op jit(solution)/shard_map/convert_element_type | solution.py:193
  211.4 7.5 %fusion.72 = f32[128,2,8,64]{3,2,1,0:T(8,128)S(1)} fusion(f32[128,2,64,64]{3,2,1,0:T(8,128)S(1)} %bitcast.315, f32[128,2,8,64]{3,0,2,1:T(8,128)S(1)} %multiply_multiply_fusion.1), kind=kOutput, calls=%fused_computation.126 | convolution fusion | flops 100663296 | bytes 5242880 | tf_op jit(solution)/shard_map/bhtk,bhkv->bhtv/dot_general | solution.py:46
  218.9 7.2 %fusion.46 = f32[128,2,8,64]{3,2,1,0:T(8,128)S(1)} fusion(f32[128,2,64,64]{3,2,1,0:T(8,128)S(1)} %bitcast.315, f32[128,2,8,64]{3,0,2,1:T(8,128)S(1)} %slice.467), kind=kOutput, calls=%fused_computation.90 | convolution fusion | flops 100663296 | bytes 5242880 | tf_op jit(solution)/shard_map/bhtk,bhkv->bhtv/dot_general | solution.py:42
  237.5 50.8 %all-gather.7.cloned.1.call-done = bf16[1024,2048]{1,0:T(8,128)(2,1)} async-done(((bf16[1024,128]{1,0:T(8,128)(2,1)}), bf16[1024,2048]{1,0:T(8,128)(2,1)}) %all-gather.7.cloned.1.call-update) | async-done | bytes 4194320 | tf_op jit(solution)/shard_map/all_gather | solution.py:128
  293.7 7.4 %copy.609 = f32[1,128,2,4096]{1,3,2,0:T(8,128)} copy(f32[1,128,2,4096]{3,2,1,0:T(2,128)} %get-tuple-element.40) | data formatting | bytes 8388608
  301.1 9.1 %copy.539 = f32[128,2,64,64]{3,2,1,0:T(8,128)} copy(f32[128,2,64,64]{0,3,2,1:T(8,128)} %bitcast.323) | data formatting | bytes 8388608 | tf_op jit(solution)/shard_map/reshape;squeeze | solution.py:99
  310.8 58.1 %all-gather.9.cloned.1.call-done = bf16[1024,4096]{1,0:T(8,128)(2,1)} async-done(((bf16[1024,256]{1,0:T(8,128)(2,1)}), bf16[1024,4096]{1,0:T(8,128)(2,1)}) %all-gather.9.cloned.1.call-update) | async-done | bytes 8388624 | tf_op jit(solution)/shard_map/all_gather | solution.py:211
  374.7 6.9 %fusion.5 = bf16[1024,4096]{1,0:T(8,128)(2,1)S(1)} fusion(bf16[1024,4096]{1,0:T(8,128)(2,1)S(1)} %copy-done.1, bf16[1024,4096]{1,0:T(8,128)(2,1)} %all-gather.5.cloned.1.call-done, f32[4096]{0:T(1024)S(1)} %bitcast.334, f32[1024]{0:T(1024)S(1)} %add_rsqrt_fusion.6), kind=kLoop, calls=%fused_computation.10 | loop fusion | flops 25165824 | bytes 25186304 | tf_op jit(solution)/shard_map/convert_element_type | solution.py:141
  386.6 10.4 %multiply_convert_fusion = bf16[1024,4096]{1,0:T(8,128)(2,1)} fusion(f32[4096]{0:T(1024)S(1)} %bitcast.335, f32[1024]{0:T(1024)S(1)} %add_rsqrt_fusion.5, bf16[1024,4096]{1,0:T(8,128)(2,1)} %copy-done), kind=kLoop, calls=%fused_computation.11 | loop fusion | flops 16777216 | bytes 16797696 | tf_op jit(solution)/shard_map/convert_element_type | solution.py:193
  411.2 6.8 %convolution_convert_fusion.2 = bf16[1024,128]{1,0:T(8,128)(2,1)} fusion(bf16[1024,4096]{1,0:T(8,128)(2,1)} %multiply_convert_fusion, bf16[2,4096,128]{2,1,0:T(8,128)(2,1)} %param.20), kind=kOutput, calls=%fused_computation.26 | convolution fusion | flops 1073872896 | bytes 9699328 | tf_op jit(solution)/shard_map/dot_general | solution.py:122
  464.3 10.4 %fusion.64 = f32[128,2,8,64]{3,2,1,0:T(8,128)} fusion(f32[128,2,64,64]{3,2,1,0:T(8,128)} %copy.539, f32[128,2,8,64]{3,0,2,1:T(8,128)S(1)} %copy-done.9), kind=kOutput, calls=%fused_computation.118 | convolution fusion | flops 100663296 | bytes 5242880 | tf_op jit(solution)/shard_map/bhtk,bhkv->bhtv/dot_general | solution.py:46
  523.9 7.2 %fusion.44 = f32[128,2,8,64]{3,2,1,0:T(8,128)S(1)} fusion(f32[128,2,64,64]{3,2,1,0:T(8,128)S(1)} %bitcast.317, f32[128,2,8,64]{3,0,2,1:T(8,128)S(1)} %slice.511), kind=kOutput, calls=%fused_computation.88 | convolution fusion | flops 100663296 | bytes 5242880 | tf_op jit(solution)/shard_map/bhtk,bhkv->bhtv/dot_general | solution.py:42
  543.0 18.4 %multiply_add_fusion.1 = f32[128,2,64,64]{3,2,1,0:T(8,128)} fusion(f32[128,2,64,64]{3,2,1,0:T(8,128)} %copy.482, f32[128,2]{1,0:T(8,128)S(1)} %bitcast.332, f32[128,2,8,64]{3,0,2,1:T(8,128)S(1)} %get-tuple-element.12, f32[128,2,8,64]{3,0,2,1:T(8,128)S(1)} %slice_subtract_fusion.1), kind=kOutput, calls=%fused_computation.15 | convolution fusion | flops 102760448 | bytes 9438208 | tf_op jit(solution)/shard_map/bhsk,bhsv->bhkv/dot_general | solution.py:51
  561.4 8.0 %copy.596 = f32[128,2,64,64]{0,3,2,1:T(8,128)} copy(f32[128,2,64,64]{3,2,1,0:T(8,128)} %multiply_add_fusion.1) | data formatting | bytes 8388608 | tf_op jit(solution)/shard_map/add | solution.py:51
  569.4 11.6 %convert_element_type.108 = f32[1024,4096]{1,0:T(8,128)} convert(bf16[1024,4096]{1,0:T(8,128)(2,1)} %copy-done) | non-fusion elementwise | flops 4194304 | bytes 25165824 | tf_op jit(solution)/shard_map/convert_element_type | solution.py:191
  582.0 18.6 %multiply_add_fusion = f32[128,2,64,64]{3,2,1,0:T(8,128)} fusion(f32[128,2,64,64]{3,2,1,0:T(8,128)} %copy.539, f32[128,2]{1,0:T(8,128)S(1)} %bitcast.333, f32[128,2,8,64]{3,0,2,1:T(8,128)S(1)} %copy-done.2, f32[128,2,8,64]{3,0,2,1:T(8,128)S(1)} %copy-done.4), kind=kOutput, calls=%fused_computation.14 | convolution fusion | flops 102760448 | bytes 9438208 | tf_op jit(solution)/shard_map/bhsk,bhsv->bhkv/dot_general | solution.py:51
  600.6 8.0 %copy.602 = f32[128,2,64,64]{0,3,2,1:T(8,128)} copy(f32[128,2,64,64]{3,2,1,0:T(8,128)} %multiply_add_fusion) | data formatting | bytes 8388608 | tf_op jit(solution)/shard_map/add | solution.py:51
  608.6 7.4 %pad_maximum_fusion = f32[2,128,2,4096]{1,3,2,0:T(8,128)} fusion(f32[1,128,2,4096]{1,3,2,0:T(8,128)} %bitcast.325, f32[1,128,2,4096]{1,3,2,0:T(8,128)} %bitcast.324), kind=kLoop, calls=%fused_computation.13 | loop fusion | flops 2097152 | bytes 16777216 | tf_op jit(solution)/shard_map/stack | solution.py:224
  616.0 13.3 %copy.603 = f32[2,128,2,4096]{3,2,1,0:T(2,128)} copy(f32[2,128,2,4096]{1,3,2,0:T(8,128)} %pad_maximum_fusion) | data formatting | bytes 16777216
  632.9 31.4 %psum.7 = f32[1024]{0:T(1024)S(1)} all-reduce(f32[1024]{0:T(1024)S(1)} %fusion.8), channel_id=1, replica_groups=mesh['grp'=2,'tp'=16] {'tp'}, use_global_device_ids=true, to_apply=%region_12.13 | all-reduce | flops 1024 | bytes 8192 | tf_op jit(solution)/shard_map/psum | solution.py:138
  (401 shorter events, 271.6 us)
Async XLA Ops:
  7.2 83.5 %all-gather.5.cloned.1.call-start = ((), (), s32[]{:S(2)}) async-start(), calls=%async_computation | async-start | bytes 8912896 | tf_op jit(solution)/shard_map/all_gather | solution.py:186
  7.9 280.4 %all-gather.7.cloned.1.call-start = ((), (), s32[]{:S(2)}) async-start(), calls=%async_computation.1 | async-start | bytes 4456448 | tf_op jit(solution)/shard_map/all_gather | solution.py:128
  33.1 10.8 %copy-start.13 = (bf16[2,4096,32]{1,2,0:T(8,128)(2,1)S(1)}, bf16[2,4096,32]{1,2,0:T(8,128)(2,1)}, u32[]{:S(2)}) copy-start(bf16[2,4096,32]{1,2,0:T(8,128)(2,1)} %param.22) | copy-start | bytes 1572868
  42.5 85.7 %copy-start.76 = (pred[8,8]{1,0:T(8,128)(4,1)}, pred[8,8]{1,0:T(8,128)(4,1)S(1)}, u32[]{:S(2)}) copy-start(pred[8,8]{1,0:T(8,128)(4,1)S(1)} %get-tuple-element.131) | copy-start | bytes 196
  42.5 85.7 %copy-start.77 = (pred[8,8]{1,0:T(8,128)(4,1)}, pred[8,8]{1,0:T(8,128)(4,1)S(1)}, u32[]{:S(2)}) copy-start(pred[8,8]{1,0:T(8,128)(4,1)S(1)} %get-tuple-element.130) | copy-start | bytes 196
  127.5 12.8 %slice-start.4 = ((s8[8388608]{0:T(1024)(128)(4,1)}), s8[4194304]{0:T(1024)(128)(4,1)S(1)}, s32[]{:S(2)}) async-start(s8[8388608]{0:T(1024)(128)(4,1)} %bitcast.318), calls=%async_computation.8 | async-start | bytes 8388608
  129.2 11.2 %slice-start.5 = ((s8[8388608]{0:T(1024)(128)(4,1)}), s8[4194304]{0:T(1024)(128)(4,1)S(1)}, s32[]{:S(2)}) async-start(s8[8388608]{0:T(1024)(128)(4,1)} %bitcast.318), calls=%async_computation.9 | async-start | bytes 8388608
  129.2 11.2 %copy-start.81 = (bf16[2,4096,128]{2,1,0:T(8,128)(2,1)S(1)}, bf16[2,4096,128]{2,1,0:T(8,128)(2,1)}, u32[]{:S(2)}) copy-start(bf16[2,4096,128]{2,1,0:T(8,128)(2,1)} %param.20) | copy-start | bytes 6291460
  232.8 60.1 %copy-start.80 = (f32[128]{0:T(128)S(1)}, f32[128]{0:T(128)}, u32[]{:S(2)}) copy-start(f32[128]{0:T(128)} %get-tuple-element.10) | copy-start | bytes 1540
  232.8 60.7 %copy-start.26 = (f32[1,128,8,2]{1,3,2,0:T(2,128)S(1)}, f32[1,128,8,2]{1,3,2,0:T(2,128)}, u32[]{:S(2)}) copy-start(f32[1,128,8,2]{1,3,2,0:T(2,128)} %get-tuple-element.119) | copy-start | bytes 24580
  237.5 131.4 %all-gather.9.cloned.1.call-start = ((), (), s32[]{:S(2)}) async-start(), calls=%async_computation.2 | async-start | bytes 8912896 | tf_op jit(solution)/shard_map/all_gather | solution.py:211
  292.9 336.4 %all-gather.11.cloned.1.call-start = ((), (), s32[]{:S(2)}) async-start(), calls=%async_computation.3 | async-start | bytes 4456448 | tf_op jit(solution)/shard_map/all_gather | solution.py:128
  397.1 12.4 %copy-start.73 = (f32[2]{0:T(128)S(1)}, f32[2]{0:T(128)}, u32[]{:S(2)}) copy-start(f32[2]{0:T(128)} %get-tuple-element.122) | copy-start | bytes 28
  397.1 12.4 %copy-start.74 = (f32[2]{0:T(128)S(1)}, f32[2]{0:T(128)}, u32[]{:S(2)}) copy-start(f32[2]{0:T(128)} %get-tuple-element.129) | copy-start | bytes 28
  410.5 23.3 %copy-start.21 = (f32[128,2,8]{2,1,0:T(2,128)}, f32[128,2,8]{2,1,0:T(2,128)S(1)}, u32[]{:S(2)}) copy-start(f32[128,2,8]{2,1,0:T(2,128)S(1)} %copy.544) | copy-start | bytes 24580
  411.2 13.4 %slice-start.6 = ((s8[8388608]{0:T(1024)(128)(4,1)}), s8[4194304]{0:T(1024)(128)(4,1)S(1)}, s32[]{:S(2)}) async-start(s8[8388608]{0:T(1024)(128)(4,1)} %bitcast.320), calls=%async_computation.10 | async-start | bytes 8388608
  434.7 11.7 %copy-start.18 = (f32[128,8,2]{1,0,2:T(8,128)S(1)}, f32[128,8,2]{1,0,2:T(8,128)}, u32[]{:S(2)}) copy-start(f32[128,8,2]{1,0,2:T(8,128)} %get-tuple-element.106) | copy-start | bytes 24580
  434.7 11.7 %copy-start.17 = (f32[128,2,8]{2,0,1:T(8,128)S(1)}, f32[128,2,8]{2,0,1:T(8,128)}, u32[]{:S(2)}) copy-start(f32[128,2,8]{2,0,1:T(8,128)} %get-tuple-element.107) | copy-start | bytes 24580
  434.7 12.4 %copy-start.16 = (f32[128,2,8]{2,0,1:T(8,128)S(1)}, f32[128,2,8]{2,0,1:T(8,128)}, u32[]{:S(2)}) copy-start(f32[128,2,8]{2,0,1:T(8,128)} %get-tuple-element.109) | copy-start | bytes 24580
  531.1 11.0 %copy-start.14 = (f32[128,2,1]{2,0,1:T(8,128)S(1)}, f32[128,2,1]{2,0,1:T(8,128)}, u32[]{:S(2)}) copy-start(f32[128,2,1]{2,0,1:T(8,128)} %get-tuple-element.102) | copy-start | bytes 3076
  569.4 11.7 %copy-start.15 = (f32[128,2,1]{2,0,1:T(8,128)S(1)}, f32[128,2,1]{2,0,1:T(8,128)}, u32[]{:S(2)}) copy-start(f32[128,2,1]{2,0,1:T(8,128)} %get-tuple-element.104) | copy-start | bytes 3076
  569.4 12.5 %copy-start.2 = (f32[128,2,8,64]{3,0,2,1:T(8,128)S(1)}, f32[128,2,8,64]{3,0,2,1:T(8,128)}, u32[]{:S(2)}) copy-start(f32[128,2,8,64]{3,0,2,1:T(8,128)} %get-tuple-element.14) | copy-start | bytes 1572868
  569.4 12.5 %copy-start.4 = (f32[128,2,8,64]{3,0,2,1:T(8,128)S(1)}, f32[128,2,8,64]{3,0,2,1:T(8,128)}, u32[]{:S(2)}) copy-start(f32[128,2,8,64]{3,0,2,1:T(8,128)} %copy-done.3) | copy-start | bytes 1572868
  616.0 13.3 %copy-start.87 = (bf16[2,2048,256]{2,1,0:T(8,128)(2,1)S(1)}, bf16[2,2048,256]{2,1,0:T(8,128)(2,1)}, u32[]{:S(2)}) copy-start(bf16[2,2048,256]{2,1,0:T(8,128)(2,1)} %param.27) | copy-start | bytes 6291460
  (77 other events, 356.0 us)
Sparse Core Ops, SparseCore 0:
  10.1 80.4 all-gather.4
  237.6 50.6 all-gather.6
  293.0 75.8 all-gather.8
  541.6 50.6 all-gather.10
where the time goes:
time: 680 us; the launch traced here: 674 us
  local copies, waits for them, and re-layouts  224 us (33%)
  matrix products  159 us (23%)
  waiting for transfers between devices  156 us (23%)
  other arithmetic  87.2 us (13%)
  blocking collectives  31.4 us (5%)
  between operations  15.9 us (2%)
    slice x60, local copies, waits for them, and re-layouts, solve_lower(): a_mat[..., row_at, col_at][..., None] * solved_rows[col_at]  95.2 us
    all_gather x1, waiting for transfers between devices, local(): gathered = lax.all_gather(mixed_out, 'tp', axis=1, tiled=True)  58.1 us
    dot_general x12, matrix products, project(): jnp.dot(portion, weight, preferred_element_type=jnp.float32)  55.6 us
    all_gather x2, waiting for transfers between devices, out_project(): lax.all_gather(blended_token_vectors, 'tp', axis=1, tiled=True)  50.8 us
    all_gather x1, waiting for transfers between devices, local(): lax.all_gather(residual_channel.reshape(row_count, own_width), 'tp', axis...  46 us
    unnamed x199, local copies, waits for them, and re-layouts  38.2 us
    dot_general x2, matrix products, delta_block(): jnp.einsum('bhsk,bhsv->bhkv', key_rows * jnp.exp(final_log - cumulative)[...  37 us
    psum x1, blocking collectives, post_residual(): squares = lax.psum(squares, 'tp')  31.4 us
  transfers between devices with their start and end apart: 4, of which 3 were waited for; matrix products, arithmetic and copies ran while one was open for 21% of the time, Pallas kernels for 0%

commit v1 on v0

--- a/solution.py
+++ b/solution.py
@@ -208,7 +208,16 @@
         mapped_token_vectors = project(hidden, weights)
         mixed_out = mix_layer(mapped_token_vectors, block_index_number)
         if block_index_number < LAYERS - 1:
-            gathered = lax.all_gather(mixed_out, "tp", axis=1, tiled=True)
+            ring = [mixed_out]
+            for hop in range(15):
+                ring.append(
+                    lax.ppermute(ring[-1], "tp", [(dev, (dev + 1) % 16) for dev in range(16)])
+                )
+            gathered = jnp.roll(
+                jnp.concatenate(ring[::-1], axis=1),
+                (lax.axis_index("tp") + 1) * ring[0].shape[1],
+                axis=1,
+            )
             whole_rows = post_residual(
                 widened, gathered, post_mixing_multiplier[block_index_number], True
             )

time: 680 us -> 810 us (1.19)
  waiting for transfers between devices: 156 us -> 251 us
  local copies, waits for them, and re-layouts: 224 us -> 285 us
  other arithmetic: 87.2 us -> 68.4 us
  matrix products: 159 us -> 149 us
    ppermute x0 -> x15, waiting for transfers between devices: none -> 158 us  [local(): lax.ppermute(ring[-1], 'tp', [(dev, (dev + 1) % 16) for dev in range(16)])]
    all_gather x1 -> x0, waiting for transfers between devices: 58.1 us -> none  [local(): gathered = lax.all_gather(mixed_out, 'tp', axis=1, tiled=True)]
    unnamed x199 -> x280, local copies, waits for them, and re-layouts: 38.2 us -> 86.6 us
    convert_element_type x2, other arithmetic: 21 us -> 4.25 us  [local(): (widened * inv_rms * prior_block_multiplier[block_index_number]).astype(j...]
    dot_general x12, matrix products: 55.6 us -> 45.9 us  [project(): jnp.dot(portion, weight, preferred_element_type=jnp.float32)]
  transfers between devices with their start and end apart: 4 -> 18, of which waited for: 3 -> 16; matrix products, arithmetic and copies ran while one was open for 21% -> 18% of each run, Pallas kernels for 0% -> 0%
where the time goes in v1:
time: 810 us; the launch traced here: 799 us
  local copies, waits for them, and re-layouts  285 us (35%)
  waiting for transfers between devices  251 us (31%)
  matrix products  149 us (18%)
  other arithmetic  68.4 us (8%)
  blocking collectives  29.5 us (4%)
  between operations  16 us (2%)
    ppermute x15, waiting for transfers between devices, local(): lax.ppermute(ring[-1], 'tp', [(dev, (dev + 1) % 16) for dev in range(16)])  158 us
    slice x60, local copies, waits for them, and re-layouts, solve_lower(): a_mat[..., row_at, col_at][..., None] * solved_rows[col_at]  95.4 us
    unnamed x280, local copies, waits for them, and re-layouts  86.6 us
    all_gather x2, waiting for transfers between devices, out_project(): lax.all_gather(blended_token_vectors, 'tp', axis=1, tiled=True)  51.2 us
    dot_general x12, matrix products, project(): jnp.dot(portion, weight, preferred_element_type=jnp.float32)  45.9 us
    all_gather x1, waiting for transfers between devices, local(): lax.all_gather(residual_channel.reshape(row_count, own_width), 'tp', axis...  41.9 us
    dot_general x2, matrix products, delta_block(): jnp.einsum('bhsk,bhsv->bhkv', key_rows * jnp.exp(final_log - cumulative)[...  36.8 us
    psum x1, blocking collectives, post_residual(): squares = lax.psum(squares, 'tp')  29.5 us
  transfers between devices with their start and end apart: 18, of which 16 were waited for; matrix products, arithmetic and copies ran while one was open for 18% of the time, Pallas kernels for 0%

profile of v1, /device:TPU:0, one launch (start us, length us, event | category | flops | bytes accessed | tf_op | source)
XLA Modules:
  0.0 798.7 jit_solution(11706103741222676552)
XLA Ops:
  12.8 14.3 %fusion.190 = (f32[1,128,2,4096]{3,2,1,0:T(2,128)}, f32[1,128,2,4096]{3,2,1,0:T(2,128)}) fusion(f32[2,128,2,4096]{3,2,1,0:T(2,128)} %param.29), kind=kLoop, calls=%fused_computation.357 | loop fusion | bytes 16777216 | tf_op jit(solution)/shard_map/slice | solution.py:176
  34.4 9.3 %copy.495 = f32[128,2,64,64]{3,2,1,0:T(8,128)} copy(f32[128,2,64,64]{0,3,2,1:T(8,128)} %bitcast.322) | data formatting | bytes 8388608 | tf_op jit(solution)/shard_map/reshape;squeeze | solution.py:99
  45.9 41.9 %all-gather.4.cloned.1.call-done = bf16[1024,4096]{0,1:T(8,128)(2,1)} async-done(((bf16[1024,256]{0,1:T(8,128)(2,1)}), bf16[1024,4096]{0,1:T(8,128)(2,1)}) %all-gather.4.cloned.1.call-update) | async-done | bytes 8388624 | tf_op jit(solution)/shard_map/all_gather | solution.py:186
  225.3 51.2 %all-gather.6.cloned.1.call-done = bf16[1024,2048]{1,0:T(8,128)(2,1)} async-done(((bf16[1024,128]{1,0:T(8,128)(2,1)}), bf16[1024,2048]{1,0:T(8,128)(2,1)}) %all-gather.6.cloned.1.call-update) | async-done | bytes 4194320 | tf_op jit(solution)/shard_map/all_gather | solution.py:128
  280.5 11.1 %collective-permute-done = bf16[1024,256]{0,1:T(8,128)(2,1)S(1)} collective-permute-done((bf16[1024,256]{0,1:T(8,128)(2,1)S(1)}, bf16[1024,256]{0,1:T(8,128)(2,1)S(1)}, u32[]{:S(2)}, u32[]{:S(2)}) %collective-permute-start) | collective-permute-done | bytes 524320 | tf_op jit(solution)/shard_map/ppermute | solution.py:214
  291.6 11.3 %collective-permute-done.1 = bf16[1024,256]{0,1:T(8,128)(2,1)S(1)} collective-permute-done((bf16[1024,256]{0,1:T(8,128)(2,1)S(1)}, bf16[1024,256]{0,1:T(8,128)(2,1)S(1)}, u32[]{:S(2)}, u32[]{:S(2)}) %collective-permute-start.1) | collective-permute-done | bytes 524320 | tf_op jit(solution)/shard_map/ppermute | solution.py:214
  303.7 11.3 %collective-permute-done.2 = bf16[1024,256]{0,1:T(8,128)(2,1)S(1)} collective-permute-done((bf16[1024,256]{0,1:T(8,128)(2,1)S(1)}, bf16[1024,256]{0,1:T(8,128)(2,1)S(1)}, u32[]{:S(2)}, u32[]{:S(2)}) %collective-permute-start.2) | collective-permute-done | bytes 524320 | tf_op jit(solution)/shard_map/ppermute | solution.py:214
  315.8 11.3 %collective-permute-done.3 = bf16[1024,256]{0,1:T(8,128)(2,1)S(1)} collective-permute-done((bf16[1024,256]{0,1:T(8,128)(2,1)S(1)}, bf16[1024,256]{0,1:T(8,128)(2,1)S(1)}, u32[]{:S(2)}, u32[]{:S(2)}) %collective-permute-start.3) | collective-permute-done | bytes 524320 | tf_op jit(solution)/shard_map/ppermute | solution.py:214
  327.9 11.3 %collective-permute-done.4 = bf16[1024,256]{0,1:T(8,128)(2,1)S(1)} collective-permute-done((bf16[1024,256]{0,1:T(8,128)(2,1)S(1)}, bf16[1024,256]{0,1:T(8,128)(2,1)S(1)}, u32[]{:S(2)}, u32[]{:S(2)}) %collective-permute-start.4) | collective-permute-done | bytes 524320 | tf_op jit(solution)/shard_map/ppermute | solution.py:214
  340.0 11.3 %collective-permute-done.5 = bf16[1024,256]{0,1:T(8,128)(2,1)S(1)} collective-permute-done((bf16[1024,256]{0,1:T(8,128)(2,1)S(1)}, bf16[1024,256]{0,1:T(8,128)(2,1)S(1)}, u32[]{:S(2)}, u32[]{:S(2)}) %collective-permute-start.5) | collective-permute-done | bytes 524320 | tf_op jit(solution)/shard_map/ppermute | solution.py:214
  352.1 11.3 %collective-permute-done.6 = bf16[1024,256]{0,1:T(8,128)(2,1)S(1)} collective-permute-done((bf16[1024,256]{0,1:T(8,128)(2,1)S(1)}, bf16[1024,256]{0,1:T(8,128)(2,1)S(1)}, u32[]{:S(2)}, u32[]{:S(2)}) %collective-permute-start.6) | collective-permute-done | bytes 524320 | tf_op jit(solution)/shard_map/ppermute | solution.py:214
  364.2 11.3 %collective-permute-done.7 = bf16[1024,256]{0,1:T(8,128)(2,1)S(1)} collective-permute-done((bf16[1024,256]{0,1:T(8,128)(2,1)S(1)}, bf16[1024,256]{0,1:T(8,128)(2,1)S(1)}, u32[]{:S(2)}, u32[]{:S(2)}) %collective-permute-start.7) | collective-permute-done | bytes 524320 | tf_op jit(solution)/shard_map/ppermute | solution.py:214
  376.3 11.3 %collective-permute-done.8 = bf16[1024,256]{0,1:T(8,128)(2,1)S(1)} collective-permute-done((bf16[1024,256]{0,1:T(8,128)(2,1)S(1)}, bf16[1024,256]{0,1:T(8,128)(2,1)S(1)}, u32[]{:S(2)}, u32[]{:S(2)}) %collective-permute-start.8) | collective-permute-done | bytes 524320 | tf_op jit(solution)/shard_map/ppermute | solution.py:214
  388.4 11.3 %collective-permute-done.9 = bf16[1024,256]{0,1:T(8,128)(2,1)S(1)} collective-permute-done((bf16[1024,256]{0,1:T(8,128)(2,1)S(1)}, bf16[1024,256]{0,1:T(8,128)(2,1)S(1)}, u32[]{:S(2)}, u32[]{:S(2)}) %collective-permute-start.9) | collective-permute-done | bytes 524320 | tf_op jit(solution)/shard_map/ppermute | solution.py:214
  400.5 11.3 %collective-permute-done.10 = bf16[1024,256]{0,1:T(8,128)(2,1)S(1)} collective-permute-done((bf16[1024,256]{0,1:T(8,128)(2,1)S(1)}, bf16[1024,256]{0,1:T(8,128)(2,1)S(1)}, u32[]{:S(2)}, u32[]{:S(2)}) %collective-permute-start.10) | collective-permute-done | bytes 524320 | tf_op jit(solution)/shard_map/ppermute | solution.py:214
  412.7 11.3 %collective-permute-done.11 = bf16[1024,256]{0,1:T(8,128)(2,1)S(1)} collective-permute-done((bf16[1024,256]{0,1:T(8,128)(2,1)S(1)}, bf16[1024,256]{0,1:T(8,128)(2,1)S(1)}, u32[]{:S(2)}, u32[]{:S(2)}) %collective-permute-start.11) | collective-permute-done | bytes 524320 | tf_op jit(solution)/shard_map/ppermute | solution.py:214
  424.7 11.4 %collective-permute-done.12 = bf16[1024,256]{0,1:T(8,128)(2,1)} collective-permute-done((bf16[1024,256]{0,1:T(8,128)(2,1)S(1)}, bf16[1024,256]{0,1:T(8,128)(2,1)}, u32[]{:S(2)}, u32[]{:S(2)}) %collective-permute-start.12) | collective-permute-done | bytes 524320 | tf_op jit(solution)/shard_map/ppermute | solution.py:214
  454.1 10.9 %collective-permute-done.14 = bf16[1024,256]{0,1:T(8,128)(2,1)S(1)} collective-permute-done((bf16[1024,256]{0,1:T(8,128)(2,1)}, bf16[1024,256]{0,1:T(8,128)(2,1)S(1)}, u32[]{:S(2)}, u32[]{:S(2)}) %collective-permute-start.14) | collective-permute-done | bytes 524320 | tf_op jit(solution)/shard_map/ppermute | solution.py:214
  590.7 10.5 %fusion.64 = f32[128,2,8,64]{3,2,1,0:T(8,128)} fusion(f32[128,2,64,64]{3,2,1,0:T(8,128)} %copy.552, f32[128,2,8,64]{3,0,2,1:T(8,128)S(1)} %copy-done.12), kind=kOutput, calls=%fused_computation.118 | convolution fusion | flops 100663296 | bytes 5242880 | tf_op jit(solution)/shard_map/bhtk,bhkv->bhtv/dot_general | solution.py:46
  669.6 18.4 %multiply_add_fusion.1 = f32[128,2,64,64]{3,2,1,0:T(8,128)} fusion(f32[128,2,64,64]{3,2,1,0:T(8,128)} %copy.495, f32[128,2]{1,0:T(8,128)S(1)} %bitcast.332, f32[128,2,8,64]{3,0,2,1:T(8,128)S(1)} %get-tuple-element.14, f32[128,2,8,64]{3,0,2,1:T(8,128)S(1)} %slice_subtract_fusion.1), kind=kOutput, calls=%fused_computation.15 | convolution fusion | flops 102760448 | bytes 9438208 | tf_op jit(solution)/shard_map/bhsk,bhsv->bhkv/dot_general | solution.py:51
  696.7 11.5 %convert_element_type.108 = f32[1024,4096]{0,1:T(8,128)} convert(bf16[1024,4096]{0,1:T(8,128)(2,1)} %copy-done) | non-fusion elementwise | flops 4194304 | bytes 25165824 | tf_op jit(solution)/shard_map/convert_element_type | solution.py:191
  709.1 18.4 %multiply_add_fusion = f32[128,2,64,64]{3,2,1,0:T(8,128)} fusion(f32[128,2,64,64]{3,2,1,0:T(8,128)} %copy.552, f32[128,2]{1,0:T(8,128)S(1)} %bitcast.333, f32[128,2,8,64]{3,0,2,1:T(8,128)S(1)} %copy-done.5, f32[128,2,8,64]{3,0,2,1:T(8,128)S(1)} %copy-done.7), kind=kOutput, calls=%fused_computation.14 | convolution fusion | flops 102760448 | bytes 9438208 | tf_op jit(solution)/shard_map/bhsk,bhsv->bhkv/dot_general | solution.py:51
  742.9 13.3 %copy.618 = f32[2,128,2,4096]{3,2,1,0:T(2,128)} copy(f32[2,128,2,4096]{1,3,2,0:T(8,128)} %pad_maximum_fusion) | data formatting | bytes 16777216
  759.8 29.5 %psum.7 = f32[1024]{0:T(1024)S(1)} all-reduce(f32[1024]{0:T(1024)S(1)} %fusion.8), channel_id=1, replica_groups=mesh['grp'=2,'tp'=16] {'tp'}, use_global_device_ids=true, to_apply=%region_12.13 | all-reduce | flops 1024 | bytes 8192 | tf_op jit(solution)/shard_map/psum | solution.py:138
  (513 shorter events, 406.8 us)
Async XLA Ops:
  7.2 80.6 %all-gather.4.cloned.1.call-start = ((), (), s32[]{:S(2)}) async-start(), calls=%async_computation | async-start | bytes 8912896 | tf_op jit(solution)/shard_map/all_gather | solution.py:186
  9.3 267.2 %all-gather.6.cloned.1.call-start = ((), (), s32[]{:S(2)}) async-start(), calls=%async_computation.1 | async-start | bytes 4456448 | tf_op jit(solution)/shard_map/all_gather | solution.py:128
  43.8 71.7 %copy-start.101 = (pred[8,8]{1,0:T(8,128)(4,1)}, pred[8,8]{1,0:T(8,128)(4,1)S(1)}, u32[]{:S(2)}) copy-start(pred[8,8]{1,0:T(8,128)(4,1)S(1)} %get-tuple-element.133) | copy-start | bytes 196
  43.8 71.7 %copy-start.102 = (pred[8,8]{1,0:T(8,128)(4,1)}, pred[8,8]{1,0:T(8,128)(4,1)S(1)}, u32[]{:S(2)}) copy-start(pred[8,8]{1,0:T(8,128)(4,1)S(1)} %get-tuple-element.132) | copy-start | bytes 196
  222.3 213.9 %copy-start.105 = (f32[128]{0:T(128)S(1)}, f32[128]{0:T(128)}, u32[]{:S(2)}) copy-start(f32[128]{0:T(128)} %get-tuple-element.12) | copy-start | bytes 1540
  222.3 214.5 %copy-start.51 = (f32[1,128,8,2]{1,3,2,0:T(2,128)S(1)}, f32[1,128,8,2]{1,3,2,0:T(2,128)}, u32[]{:S(2)}) copy-start(f32[1,128,8,2]{1,3,2,0:T(2,128)} %get-tuple-element.121) | copy-start | bytes 24580
  225.2 531.0 %all-gather.8.cloned.1.call-start = ((), (), s32[]{:S(2)}) async-start(), calls=%async_computation.2 | async-start | bytes 4456448 | tf_op jit(solution)/shard_map/all_gather | solution.py:128
  280.2 11.4 %collective-permute-start = (bf16[1024,256]{0,1:T(8,128)(2,1)S(1)}, bf16[1024,256]{0,1:T(8,128)(2,1)S(1)}, u32[]{:S(2)}, u32[]{:S(2)}) collective-permute-start(bf16[1024,256]{0,1:T(8,128)(2,1)S(1)} %convolution_convert_fusion.1), channel_id=1, source_target_pairs={{0,1},{1,2},{2,3},{3,4},{4,5},{5,6},{6,7},{7,8},{8,9},{9,10},{10,1... | collective-permute-start | bytes 1572872 | tf_op jit(solution)/shard_map/ppermute | solution.py:214
  291.6 11.3 %collective-permute-start.1 = (bf16[1024,256]{0,1:T(8,128)(2,1)S(1)}, bf16[1024,256]{0,1:T(8,128)(2,1)S(1)}, u32[]{:S(2)}, u32[]{:S(2)}) collective-permute-start(bf16[1024,256]{0,1:T(8,128)(2,1)S(1)} %collective-permute-done), channel_id=1, source_target_pairs={{0,1},{1,2},{2,3},{3,4},{4,5},{5,6},{6,7},{7,8},{8,9},{9,10},{10,1... | collective-permute-start | bytes 1572872 | tf_op jit(solution)/shard_map/ppermute | solution.py:214
  303.7 11.3 %collective-permute-start.2 = (bf16[1024,256]{0,1:T(8,128)(2,1)S(1)}, bf16[1024,256]{0,1:T(8,128)(2,1)S(1)}, u32[]{:S(2)}, u32[]{:S(2)}) collective-permute-start(bf16[1024,256]{0,1:T(8,128)(2,1)S(1)} %collective-permute-done.1), channel_id=1, source_target_pairs={{0,1},{1,2},{2,3},{3,4},{4,5},{5,6},{6,7},{7,8},{8,9},{9,10},{10,1... | collective-permute-start | bytes 1572872 | tf_op jit(solution)/shard_map/ppermute | solution.py:214
  315.8 11.3 %collective-permute-start.3 = (bf16[1024,256]{0,1:T(8,128)(2,1)S(1)}, bf16[1024,256]{0,1:T(8,128)(2,1)S(1)}, u32[]{:S(2)}, u32[]{:S(2)}) collective-permute-start(bf16[1024,256]{0,1:T(8,128)(2,1)S(1)} %collective-permute-done.2), channel_id=1, source_target_pairs={{0,1},{1,2},{2,3},{3,4},{4,5},{5,6},{6,7},{7,8},{8,9},{9,10},{10,1... | collective-permute-start | bytes 1572872 | tf_op jit(solution)/shard_map/ppermute | solution.py:214
  327.9 11.3 %collective-permute-start.4 = (bf16[1024,256]{0,1:T(8,128)(2,1)S(1)}, bf16[1024,256]{0,1:T(8,128)(2,1)S(1)}, u32[]{:S(2)}, u32[]{:S(2)}) collective-permute-start(bf16[1024,256]{0,1:T(8,128)(2,1)S(1)} %collective-permute-done.3), channel_id=1, source_target_pairs={{0,1},{1,2},{2,3},{3,4},{4,5},{5,6},{6,7},{7,8},{8,9},{9,10},{10,1... | collective-permute-start | bytes 1572872 | tf_op jit(solution)/shard_map/ppermute | solution.py:214
  340.0 11.3 %collective-permute-start.5 = (bf16[1024,256]{0,1:T(8,128)(2,1)S(1)}, bf16[1024,256]{0,1:T(8,128)(2,1)S(1)}, u32[]{:S(2)}, u32[]{:S(2)}) collective-permute-start(bf16[1024,256]{0,1:T(8,128)(2,1)S(1)} %collective-permute-done.4), channel_id=1, source_target_pairs={{0,1},{1,2},{2,3},{3,4},{4,5},{5,6},{6,7},{7,8},{8,9},{9,10},{10,1... | collective-permute-start | bytes 1572872 | tf_op jit(solution)/shard_map/ppermute | solution.py:214
  352.1 11.3 %collective-permute-start.6 = (bf16[1024,256]{0,1:T(8,128)(2,1)S(1)}, bf16[1024,256]{0,1:T(8,128)(2,1)S(1)}, u32[]{:S(2)}, u32[]{:S(2)}) collective-permute-start(bf16[1024,256]{0,1:T(8,128)(2,1)S(1)} %collective-permute-done.5), channel_id=1, source_target_pairs={{0,1},{1,2},{2,3},{3,4},{4,5},{5,6},{6,7},{7,8},{8,9},{9,10},{10,1... | collective-permute-start | bytes 1572872 | tf_op jit(solution)/shard_map/ppermute | solution.py:214
  364.2 11.3 %collective-permute-start.7 = (bf16[1024,256]{0,1:T(8,128)(2,1)S(1)}, bf16[1024,256]{0,1:T(8,128)(2,1)S(1)}, u32[]{:S(2)}, u32[]{:S(2)}) collective-permute-start(bf16[1024,256]{0,1:T(8,128)(2,1)S(1)} %collective-permute-done.6), channel_id=1, source_target_pairs={{0,1},{1,2},{2,3},{3,4},{4,5},{5,6},{6,7},{7,8},{8,9},{9,10},{10,1... | collective-permute-start | bytes 1572872 | tf_op jit(solution)/shard_map/ppermute | solution.py:214
  376.3 11.3 %collective-permute-start.8 = (bf16[1024,256]{0,1:T(8,128)(2,1)S(1)}, bf16[1024,256]{0,1:T(8,128)(2,1)S(1)}, u32[]{:S(2)}, u32[]{:S(2)}) collective-permute-start(bf16[1024,256]{0,1:T(8,128)(2,1)S(1)} %collective-permute-done.7), channel_id=1, source_target_pairs={{0,1},{1,2},{2,3},{3,4},{4,5},{5,6},{6,7},{7,8},{8,9},{9,10},{10,1... | collective-permute-start | bytes 1572872 | tf_op jit(solution)/shard_map/ppermute | solution.py:214
  388.4 11.3 %collective-permute-start.9 = (bf16[1024,256]{0,1:T(8,128)(2,1)S(1)}, bf16[1024,256]{0,1:T(8,128)(2,1)S(1)}, u32[]{:S(2)}, u32[]{:S(2)}) collective-permute-start(bf16[1024,256]{0,1:T(8,128)(2,1)S(1)} %collective-permute-done.8), channel_id=1, source_target_pairs={{0,1},{1,2},{2,3},{3,4},{4,5},{5,6},{6,7},{7,8},{8,9},{9,10},{10,1... | collective-permute-start | bytes 1572872 | tf_op jit(solution)/shard_map/ppermute | solution.py:214
  400.5 11.3 %collective-permute-start.10 = (bf16[1024,256]{0,1:T(8,128)(2,1)S(1)}, bf16[1024,256]{0,1:T(8,128)(2,1)S(1)}, u32[]{:S(2)}, u32[]{:S(2)}) collective-permute-start(bf16[1024,256]{0,1:T(8,128)(2,1)S(1)} %collective-permute-done.9), channel_id=1, source_target_pairs={{0,1},{1,2},{2,3},{3,4},{4,5},{5,6},{6,7},{7,8},{8,9},{9,10},{10,1... | collective-permute-start | bytes 1572872 | tf_op jit(solution)/shard_map/ppermute | solution.py:214
  412.6 11.3 %collective-permute-start.11 = (bf16[1024,256]{0,1:T(8,128)(2,1)S(1)}, bf16[1024,256]{0,1:T(8,128)(2,1)S(1)}, u32[]{:S(2)}, u32[]{:S(2)}) collective-permute-start(bf16[1024,256]{0,1:T(8,128)(2,1)S(1)} %collective-permute-done.10), channel_id=1, source_target_pairs={{0,1},{1,2},{2,3},{3,4},{4,5},{5,6},{6,7},{7,8},{8,9},{9,10},{10,1... | collective-permute-start | bytes 1572872 | tf_op jit(solution)/shard_map/ppermute | solution.py:214
  424.7 11.4 %collective-permute-start.12 = (bf16[1024,256]{0,1:T(8,128)(2,1)S(1)}, bf16[1024,256]{0,1:T(8,128)(2,1)}, u32[]{:S(2)}, u32[]{:S(2)}) collective-permute-start(bf16[1024,256]{0,1:T(8,128)(2,1)S(1)} %collective-permute-done.11), channel_id=1, source_target_pairs={{0,1},{1,2},{2,3},{3,4},{4,5},{5,6},{6,7},{7,8},{8,9},{9,10},{10,1... | collective-permute-start | bytes 1572872 | tf_op jit(solution)/shard_map/ppermute | solution.py:214
  436.2 17.2 %collective-permute-start.13 = (bf16[1024,256]{0,1:T(8,128)(2,1)}, bf16[1024,256]{0,1:T(8,128)(2,1)}, u32[]{:S(2)}, u32[]{:S(2)}) collective-permute-start(bf16[1024,256]{0,1:T(8,128)(2,1)} %collective-permute-done.12), channel_id=1, source_target_pairs={{0,1},{1,2},{2,3},{3,4},{4,5},{5,6},{6,7},{7,8},{8,9},{9,10},{10,1... | collective-permute-start | bytes 1572872 | tf_op jit(solution)/shard_map/ppermute | solution.py:214
  453.4 29.3 %copy-start.18 = (bf16[1024,256]{0,1:T(8,128)(2,1)S(1)}, bf16[1024,256]{0,1:T(8,128)(2,1)}, u32[]{:S(2)}) copy-start(bf16[1024,256]{0,1:T(8,128)(2,1)} %copy-done.17) | copy-start | bytes 1572868
  453.4 30.2 %copy-start.16 = (bf16[1024,256]{0,1:T(8,128)(2,1)S(1)}, bf16[1024,256]{0,1:T(8,128)(2,1)}, u32[]{:S(2)}) copy-start(bf16[1024,256]{0,1:T(8,128)(2,1)} %copy-done.15) | copy-start | bytes 1572868
  453.4 11.6 %collective-permute-start.14 = (bf16[1024,256]{0,1:T(8,128)(2,1)}, bf16[1024,256]{0,1:T(8,128)(2,1)S(1)}, u32[]{:S(2)}, u32[]{:S(2)}) collective-permute-start(bf16[1024,256]{0,1:T(8,128)(2,1)} %collective-permute-done.13), channel_id=1, source_target_pairs={{0,1},{1,2},{2,3},{3,4},{4,5},{5,6},{6,7},{7,8},{8,9},{9,10},{10,1... | collective-permute-start | bytes 1572872 | tf_op jit(solution)/shard_map/ppermute | solution.py:214
  (116 other events, 793.8 us)
Sparse Core Ops, SparseCore 0:
  10.7 77.0 all-gather.3
  225.4 51.0 all-gather.5
  668.2 49.7 all-gather.7
